TPU v7x, 32 devices: a whole 2x2x4 slice. The times are simulated.
32 devices in a mesh: grp: 2 (over y), sp: 4 (over z), tp: 4 (over x, core).
Axes of the slice: x: 2, y: 2, z: 4, core: 2. Of those that a mesh axis runs over, the one named last changes fastest.
Arguments:
- latent: bfloat16 [4096, 4096], P(('grp', 'sp', 'tp')), parts along dimension 0, may hold values from -260 to 260
- context: bfloat16 [1536, 4096], P(('grp', 'sp')), parts along dimension 0, may hold values from -6 to 6
- conditioning: bfloat16 [8192], P(('grp', 'sp')), parts along dimension 0, may hold values from -6 to 6
- norm_gain: float32 [4096], replicated, may hold values from 0.1 to 1.9
- shift_weight: bfloat16 [4096, 4096], P('sp', 'tp'), may hold values from -0.09375 to 0.09375
- scale_weight: bfloat16 [4096, 4096], P('sp', 'tp'), may hold values from -0.09375 to 0.09375
- gate_weight: bfloat16 [4096, 4096], P('sp', 'tp'), may hold values from -0.09375 to 0.09375
- query_weight: bfloat16 [4096, 1024], P(None, 'tp'), may hold values from -3 to 3
- key_weight: bfloat16 [4096, 512], P(None, 'tp'), may hold values from -3 to 3
- value_weight: bfloat16 [4096, 512], P(None, 'tp'), may hold values from -0.09375 to 0.09375
- out_weight: bfloat16 [1024, 4096], P(None, 'tp'), may hold values from -1.5 to 1.5
- sink_logit: float32 [16], P('tp'), may hold values from 3 to 7
Outputs:
- mixed: bfloat16 [4096, 4096], P(('grp', 'sp', 'tp')), parts along dimension 0
There are 2 independent parts, one for each index of `grp`. A program takes and returns all parts, laid end to end along the dimension named above; an argument that names none is the same for every part. Nothing has to cross between parts.
All inputs are finite; a program needn't handle non-finite values.
Results may differ from a plain program's by a relative error of at most 0.012.
The roundings to bfloat16 on the way count: a program that leaves them out, or rounds other values in their place, can miss the bound.
Values may be sent and summed in bfloat16 or wider, within the bound.
No kernel may reach another device: no remote copies, remote signals or barrier semaphores. Data moves between devices by JAX's collectives and lax.ppermute only.
A program may use at most 64 MiB of HBM per device.

v0:
```python
import functools

import jax
import jax.numpy as jnp
from jax import lax
from jax.experimental import pallas as pl
from jax.experimental.pallas import tpu as pltpu
from jax.sharding import PartitionSpec as P

HEADS = 16
KV_HEADS = 8
HD = 64
GRID_W = 64
WIN = 128
LANES = 128
CORES = 2

epsilon = 1e-06
rope_base = 10000.0
neg_large = -1e30


VMEM = pl.BlockSpec(memory_space=pltpu.VMEM)
SMEM = pl.BlockSpec(memory_space=pltpu.SMEM)


def cost(flops, traffic):
    return pl.CostEstimate(flops=int(flops), bytes_accessed=int(traffic), transcendentals=0)


def from_chip(block, count, step):
    chips = count // CORES
    perm = [
        (((t // CORES + step) % chips) * CORES + t % CORES, t) for t in range(count)
    ]
    return lax.ppermute(block, "tp", perm)


def from_partner(block, count):
    return lax.ppermute(block, "tp", [(t ^ 1, t) for t in range(count)])


def send_rows(block, count, step, flip):
    chips = count // CORES
    perm = [
        (t, ((t // CORES + step) % chips) * CORES + (t % CORES) ^ flip) for t in range(count)
    ]
    return lax.ppermute(block, "tp", perm)


def turn_tables(position):
    lane = jnp.arange(LANES, dtype=jnp.int32)
    quarter = HD // 4
    inverse = rope_base ** (-(lane % quarter).astype(jnp.float32) / quarter)
    by_row = (lane % HD) < HD // 2
    coordinate = jnp.where(
        by_row[None, :], (position // GRID_W)[:, None], (position % GRID_W)[:, None]
    )
    angles = coordinate.astype(jnp.float32) * inverse[None, :]
    sign = jnp.where(lane % (HD // 2) < quarter, -1.0, 1.0)
    return jnp.cos(angles), jnp.sin(angles) * sign[None, :]


def row_root(ref, step):
    rows, depth = ref.shape
    total = jnp.zeros((rows, LANES), jnp.float32)
    for k in range(0, depth, step):
        v = ref[:, k : k + step].astype(jnp.float32)
        v = v * v
        for c in range(0, step, LANES):
            total = total + v[:, c : c + LANES]
    return lax.rsqrt(jnp.sum(total, axis=1, keepdims=True) / depth + epsilon)


def context_kernel(context, gain, wk, wv, out):
    depth = wk.shape[0]
    step = min(depth, 512)
    root = row_root(context, step)
    acc = jnp.zeros(out.shape, jnp.float32)
    for k in range(0, depth, step):
        v = context[:, k : k + step].astype(jnp.float32) * root * gain[:, k : k + step]
        wkv = jnp.concatenate([wk[k : k + step, :], wv[k : k + step, :]], axis=1)
        acc = acc + jnp.dot(v.astype(jnp.bfloat16), wkv, preferred_element_type=jnp.float32)
    out[...] = acc.astype(jnp.bfloat16)


def project_kernel(parts, carried, place, *refs):
    x_refs = refs[:parts]
    gain, shift, wq, wk, wv, cosine, sine = refs[parts : parts + 7]
    rest = refs[parts + 7 :]
    if carried:
        q_prev, kv_prev, q_out, kv_out = rest
        q_out[...] = q_prev[...]
        kv_out[...] = kv_prev[...]
    else:
        q_out, kv_out = rest
    depth = wq.shape[0]
    step = min(depth, 512)
    rows = x_refs[0].shape[0]
    query_width = wq.shape[1]
    key_width = wk.shape[1]
    roots = []
    for ref in x_refs:
        roots.append(row_root(ref, step))
    acc_q = jnp.zeros((rows * parts, query_width), jnp.float32)
    acc_kv = jnp.zeros((rows * parts, 2 * key_width), jnp.float32)
    for k in range(0, depth, step):
        pieces = []
        for ref, root in zip(x_refs, roots):
            v = ref[:, k : k + step].astype(jnp.float32) * root
            v = v * gain[:, k : k + step] + shift[:, k : k + step]
            pieces.append(v.astype(jnp.bfloat16))
        normed = jnp.concatenate(pieces, axis=0)
        acc_q = acc_q + jnp.dot(
            normed, wq[k : k + step, :], preferred_element_type=jnp.float32
        )
        wkv = jnp.concatenate([wk[k : k + step, :], wv[k : k + step, :]], axis=1)
        acc_kv = acc_kv + jnp.dot(normed, wkv, preferred_element_type=jnp.float32)
    lane = lax.broadcasted_iota(jnp.int32, (rows, LANES), 1)
    first = lane % (HD // 2) < HD // 4
    for i in range(parts):
        start = pl.multiple_of(place[i], 16)
        cos_rows = cosine[pl.ds(start, rows), :]
        sin_rows = sine[pl.ds(start, rows), :]
        for acc, out, width in (
            (acc_q, q_out, query_width),
            (acc_kv, kv_out, key_width),
        ):
            block = acc[i * rows : (i + 1) * rows]
            for c in range(0, block.shape[1], LANES):
                piece = block[:, c : c + LANES]
                turned = min(max(width - c, 0), LANES)
                if turned:
                    other = jnp.where(
                        first,
                        pltpu.roll(piece, LANES - HD // 4, 1),
                        pltpu.roll(piece, HD // 4, 1),
                    )
                    moved = piece * cos_rows + other * sin_rows
                    piece = moved if turned == LANES else jnp.where(lane < turned, moved, piece)
                out[pl.ds(start, rows), c : c + LANES] = piece.astype(jnp.bfloat16)


def project(blocks, places, gain, shift, wq, wk, wv, tables, carried, out_rows):
    parts = len(blocks)
    depth, query_width = wq.shape
    kv_width = 2 * wk.shape[1]
    rows = blocks[0].shape[0] * parts
    return pl.pallas_call(
        functools.partial(project_kernel, parts, bool(carried)),
        out_shape=(
            jax.ShapeDtypeStruct((out_rows, query_width), jnp.bfloat16),
            jax.ShapeDtypeStruct((out_rows, kv_width), jnp.bfloat16),
        ),
        in_specs=[SMEM] + [VMEM] * (parts + 7 + len(carried)),
        out_specs=(VMEM, VMEM),
        compiler_params=pltpu.CompilerParams(vmem_limit_bytes=24 * 1024 * 1024),
        cost_estimate=cost(
            2 * rows * depth * (query_width + kv_width), 2 * depth * (rows + query_width + kv_width)
        ),
    )(jnp.stack(places), *blocks, gain, shift, wq, wk, wv, *tables, *carried)


def attend_block(q, band, ctx_refs, sink, out, out_row, low, high):
    key_width = ctx_refs[0].shape[1] // 2
    group = HEADS // KV_HEADS
    row = lax.broadcasted_iota(jnp.int32, (WIN, WIN), 0)
    col = lax.broadcasted_iota(jnp.int32, (WIN, WIN), 1)
    before = col >= row
    after = col <= row
    if low is not None:
        before = before & (low != 0)
    if high is not None:
        after = after & (high != 0)
    before = jnp.concatenate([before] * group, axis=0)
    after = jnp.concatenate([after] * group, axis=0)
    contract = (((1,), (1,)), ((), ()))
    for head in range(key_width // HD):
        base = head * group * HD
        query = jnp.concatenate(
            [q[:, base + g * HD : base + (g + 1) * HD] for g in range(group)], axis=0
        )
        query = query * jnp.asarray(HD**-0.5, jnp.bfloat16)
        ks = slice(head * HD, (head + 1) * HD)
        vs = slice(key_width + head * HD, key_width + (head + 1) * HD)
        scores = [
            lax.dot_general(
                query, ref[r : r + WIN, ks], contract, preferred_element_type=jnp.float32
            )
            for ref, r in band
        ] + [
            lax.dot_general(query, ref[:, ks], contract, preferred_element_type=jnp.float32)
            for ref in ctx_refs
        ]
        scores[0] = jnp.where(before, scores[0], neg_large)
        scores[2] = jnp.where(after, scores[2], neg_large)
        sinks = jnp.concatenate(
            [jnp.full((WIN, 1), sink[head * group + g], jnp.float32) for g in range(group)], axis=0
        )
        top = sinks
        for s in scores:
            top = jnp.maximum(top, jnp.max(s, axis=1, keepdims=True))
        values = [ref[r : r + WIN, vs] for ref, r in band] + [ref[:, vs] for ref in ctx_refs]
        gathered = jnp.zeros((group * WIN, 2 * HD), jnp.float32)
        for s, v in zip(scores, values):
            power = jnp.exp(s - top).astype(jnp.bfloat16)
            joined = jnp.concatenate([v, jnp.ones_like(v)], axis=1)
            gathered = gathered + jnp.dot(power, joined, preferred_element_type=jnp.float32)
        total = gathered[:, HD : HD + 1] + jnp.exp(sinks - top)
        gathered = gathered[:, :HD] * (1.0 / total)
        for g in range(group):
            out[out_row : out_row + WIN, base + g * HD : base + (g + 1) * HD] = gathered[
                g * WIN : (g + 1) * WIN
            ].astype(jnp.bfloat16)


def inner_kernel(blocks, sink, q, kv, *refs):
    ctx, out = refs[:-1], refs[-1]
    for n in range(1, blocks - 1):
        band = [(kv, (n + s) * WIN) for s in (-1, 0, 1)]
        attend_block(
            q[n * WIN : (n + 1) * WIN, :], band, ctx, sink, out, (n - 1) * WIN, None, None
        )


def edge_kernel(blocks, inner, ends, sink, q, kv, head, tail, *refs):
    if inner:
        ctx, middle, out = refs[:-2], refs[-2], refs[-1]
        out[WIN : (blocks - 1) * WIN, :] = middle[...]
    else:
        ctx, out = refs[:-1], refs[-1]
    for n in sorted({0, blocks - 1}):
        band = [
            (head, 0) if n == 0 else (kv, (n - 1) * WIN),
            (kv, n * WIN),
            (tail, 0) if n == blocks - 1 else (kv, (n + 1) * WIN),
        ]
        attend_block(
            q[n * WIN : (n + 1) * WIN, :],
            band,
            ctx,
            sink,
            out,
            n * WIN,
            ends[0] if n == 0 else None,
            ends[1] if n == blocks - 1 else None,
        )


def attend_cost(blocks, query_width, ctx):
    keys = 3 * WIN + sum(c.shape[0] for c in ctx)
    return cost(4 * blocks * WIN * keys * query_width * 4, 2**20)


def out_kernel(parts, rows, place, *refs):
    att, weight, outs = refs[:parts], refs[parts], refs[parts + 1 :]
    width = att[0].shape[1]
    for i in range(len(outs)):
        start = pl.multiple_of(place[i], 16)
        total = jnp.zeros((rows, weight.shape[1]), jnp.float32)
        for k in range(parts):
            total = total + jnp.dot(
                att[k][pl.ds(start, rows), :],
                weight[k * width : (k + 1) * width, :],
                preferred_element_type=jnp.float32,
            )
        outs[i][...] = total.astype(jnp.bfloat16)


def out_rows(att, weight, places, rows):
    parts = len(att)
    count = len(places)
    return pl.pallas_call(
        functools.partial(out_kernel, parts, rows),
        out_shape=tuple(
            jax.ShapeDtypeStruct((rows, weight.shape[1]), jnp.bfloat16) for _ in range(count)
        ),
        in_specs=[SMEM] + [VMEM] * (parts + 1),
        out_specs=tuple(VMEM for _ in range(count)),
        compiler_params=pltpu.CompilerParams(vmem_limit_bytes=16 * 1024 * 1024),
        cost_estimate=cost(2 * rows * count * weight.shape[0] * weight.shape[1], 2**22),
    )(jnp.stack(places), *att, weight)


def finish_kernel(place, latent, gate, blend, *refs):
    refs[-1][...] = (
        latent[...].astype(jnp.float32) + gate[...] * blend[...].astype(jnp.float32)
    ).astype(jnp.bfloat16)


def finish(latent, gate, blend, place, mixed):
    rows, width = blend.shape
    there = pl.BlockSpec((rows, width), lambda i, place: (0, place[0]))
    here = pl.BlockSpec((rows, width), lambda i, place: (0, 0))
    line = pl.BlockSpec((1, width), lambda i, place: (0, place[0]))
    return pl.pallas_call(
        finish_kernel,
        out_shape=jax.ShapeDtypeStruct(latent.shape, jnp.bfloat16),
        grid_spec=pltpu.PrefetchScalarGridSpec(
            num_scalar_prefetch=1,
            grid=(1,),
            in_specs=[there, line, here] + [pl.BlockSpec(memory_space=pl.ANY)] * len(mixed),
            out_specs=there,
        ),
        input_output_aliases={4: 0} if mixed else {},
        compiler_params=pltpu.CompilerParams(vmem_limit_bytes=8 * 1024 * 1024),
        cost_estimate=cost(2**20, 2**20),
    )(place[None], latent, gate, blend, *mixed)


def local(
    latent,
    context,
    conditioning,
    norm_gain,
    shift_weight,
    scale_weight,
    gate_weight,
    query_weight,
    key_weight,
    value_weight,
    out_weight,
    sink_logit,
):
    count = lax.axis_size("tp")
    chips = count // CORES
    me = lax.axis_index("tp")
    chip, core = me // CORES, me % CORES
    ring = lax.axis_size("sp")
    rank = lax.axis_index("sp")
    rows, depth = latent.shape
    row_count = rows * count
    cuts = 2
    piece = rows // cuts

    def index(step, flip):
        return ((chip + step) % chips) * CORES + (core ^ flip)

    near = [latent, from_partner(latent, count)]
    near_place = [index(0, 0) * rows, index(0, 1) * rows]
    far, far_place = [], []
    for step in range(1, chips):
        for cut in range(cuts):
            got = from_chip(latent[cut * piece : (cut + 1) * piece], count, step)
            far += [got, from_partner(got, count)]
            far_place += [index(step, flip) * rows + cut * piece for flip in (0, 1)]

    lifted = jax.nn.silu(conditioning.astype(jnp.float32)).astype(jnp.bfloat16)[None, :]
    partial = jnp.concatenate(
        [
            jnp.dot(lifted, w, preferred_element_type=jnp.float32)
            for w in (shift_weight, scale_weight, gate_weight)
        ],
        axis=0,
    )
    summed = jnp.sum(lax.all_gather(partial, "sp", axis=0), axis=0)
    vectors = lax.all_gather(summed, "tp", axis=1, tiled=True)
    vectors, context, rank = lax.optimization_barrier((vectors, context, rank))
    shift_vec = vectors[0:1]
    gain_vec = norm_gain[None, :] * (1.0 + vectors[1:2])
    gate_vec = vectors[2:3]

    own = pl.pallas_call(
        context_kernel,
        out_shape=jax.ShapeDtypeStruct((context.shape[0], 2 * key_weight.shape[1]), jnp.bfloat16),
        in_specs=[VMEM] * 4,
        out_specs=VMEM,
        compiler_params=pltpu.CompilerParams(vmem_limit_bytes=16 * 1024 * 1024),
        cost_estimate=cost(4 * context.shape[0] * depth * key_weight.shape[1], 2**22),
    )(context, norm_gain[None, :], key_weight, value_weight)
    if ring <= 8:
        ctx = [own] + [
            lax.ppermute(own, "sp", [((i + d) % ring, i) for i in range(ring)])
            for d in range(1, ring)
        ]
    else:
        ctx = [lax.all_gather(own, "sp", axis=0, tiled=True)]

    row_offset = rank * row_count
    tables = turn_tables(row_offset + jnp.arange(row_count, dtype=jnp.int32))
    args = (gain_vec, shift_vec, query_weight, key_weight, value_weight, tables)
    queries, key_value = project(near, near_place, *args, (), row_count)
    if far:
        queries, key_value = project(
            far, far_place, *args, (queries, key_value), row_count
        )

    head = lax.ppermute(
        key_value[row_count - WIN :], "sp", [(i, i + 1) for i in range(ring - 1)]
    )
    tail = lax.ppermute(key_value[:WIN], "sp", [(i + 1, i) for i in range(ring - 1)])
    blocks = row_count // WIN
    query_width = query_weight.shape[1]
    limit = pltpu.CompilerParams(vmem_limit_bytes=16 * 1024 * 1024)
    middle = ()
    if blocks > 2:
        middle = (
            pl.pallas_call(
                functools.partial(inner_kernel, blocks),
                out_shape=jax.ShapeDtypeStruct(((blocks - 2) * WIN, query_width), jnp.bfloat16),
                in_specs=[SMEM] + [VMEM] * (2 + len(ctx)),
                out_specs=VMEM,
                compiler_params=limit,
                cost_estimate=attend_cost(blocks - 2, query_width, ctx),
            )(sink_logit, queries, key_value, *ctx),
        )
    ends = jnp.stack([(rank > 0).astype(jnp.int32), (rank < ring - 1).astype(jnp.int32)])
    attended = pl.pallas_call(
        functools.partial(edge_kernel, blocks, bool(middle)),
        out_shape=jax.ShapeDtypeStruct((row_count, query_width), jnp.bfloat16),
        in_specs=[SMEM, SMEM] + [VMEM] * (4 + len(ctx) + len(middle)),
        out_specs=VMEM,
        compiler_params=limit,
        cost_estimate=attend_cost(2, query_width, ctx),
    )(ends, sink_logit, queries, key_value, head, tail, *ctx, *middle)

    att, order = [], []
    for step in range(chips):
        got = attended if step == 0 else from_chip(attended, count, step)
        att += [got, from_partner(got, count)]
        order += [index(step, 0), index(step, 1)]
    weight = jnp.concatenate(
        [
            lax.dynamic_slice_in_dim(out_weight, source * query_width, query_width, 0)
            for source in order
        ],
        axis=0,
    )

    steps = [(step, flip) for step in range(1, chips) for flip in range(CORES)]
    received, places = [], []
    if steps:
        sent = out_rows(att, weight, [index(s, f) * rows for s, f in steps], rows)
        for (s, f), block in zip(steps, sent):
            received.append(send_rows(block, count, s, f))
            places.append((((chip - s) % chips) * CORES + (core ^ f)) )
    mine, other = out_rows(att, weight, [index(0, 0) * rows, index(0, 1) * rows], rows)
    near_blends = [(mine, index(0, 0)), (from_partner(other, count), index(0, 1))]
    mixed = ()
    for block, place in near_blends + list(zip(received, places)):
        mixed = (finish(latent, gate_vec, block, place, mixed),)
    return mixed[0]


def solution(mesh):
    in_specs = (
        P(("grp", "sp", "tp"), None),
        P(("grp", "sp"), None),
        P(("grp", "sp")),
        P(),
        P("sp", "tp"),
        P("sp", "tp"),
        P("sp", "tp"),
        P(None, "tp"),
        P(None, "tp"),
        P(None, "tp"),
        P(None, "tp"),
        P("tp"),
    )
    out_specs = P(("grp", "sp", "tp"), None)

    return jax.shard_map(local, mesh=mesh, in_specs=in_specs, out_specs=out_specs, check_vma=False)
```

profile of v0, /device:TPU:0, one launch (start us, length us, event | category | flops | bytes accessed | tf_op | source)
XLA Modules:
  0.0 118.5 jit_solution(6301676682084037212)
XLA Ops:
  3.8 15.1 %all-gather.1 = f32[4,3,1024]{2,1,0:T(4,128)S(1)} all-gather(f32[1,3,1024]{2,1,0:T(4,128)S(1)} %maximum_bitcast_fusion), channel_id=2, replica_groups=mesh['grp'=2,'sp'=4,'tp'=4] {'sp'}, dimensions={0}, use_global_device_ids=true | all-gather | bytes 61440 | tf_op jit(solution)/shard_map/all_gather | solution.py:356
  18.8 5.7 %all_gather.11 = f32[3,4096]{1,0:T(4,128)} all-gather(f32[3,1024]{1,0:T(4,128)S(1)} %reduce_sum.9), channel_id=1, replica_groups=mesh['grp'=2,'sp'=4,'tp'=4] {'tp'}, dimensions={1}, use_global_device_ids=true | all-gather | bytes 61440 | tf_op jit(solution)/shard_map/all_gather | solution.py:357
  29.3 1.7 %collective-permute-start.9 = (bf16[192,256]{1,0:T(8,128)(2,1)S(1)}, bf16[192,256]{1,0:T(8,128)(2,1)S(1)}, u32[]{:S(2)}, u32[]{:S(2)}) collective-permute-start(bf16[192,256]{1,0:T(8,128)(2,1)S(1)} %shard_map.120.refs_0_), channel_id=1, source_target_pairs={{12,0},{0,4},{4,8},{8,12},{13,1},{1,5},{5,9},{9,13},{14,2},{2,6},{... | collective-permute-start | bytes 294920 | tf_op jit(solution)/shard_map/ppermute | solution.py:373
  31.0 2.4 %collective-permute-start.8 = (bf16[192,256]{1,0:T(8,128)(2,1)S(1)}, bf16[192,256]{1,0:T(8,128)(2,1)S(1)}, u32[]{:S(2)}, u32[]{:S(2)}) collective-permute-start(bf16[192,256]{1,0:T(8,128)(2,1)S(1)} %shard_map.120.refs_0_), channel_id=1, source_target_pairs={{8,0},{12,4},{0,8},{4,12},{9,1},{13,5},{1,9},{5,13},{10,2},{14,6},... | collective-permute-start | bytes 294920 | tf_op jit(solution)/shard_map/ppermute | solution.py:373
  34.5 1.5 %collective-permute-start.2 = (bf16[64,4096]{1,0:T(8,128)(2,1)}, bf16[64,4096]{1,0:T(8,128)(2,1)}, u32[]{:S(2)}, u32[]{:S(2)}) collective-permute-start(bf16[64,4096]{1,0:T(8,128)(2,1)} %get-tuple-element.31), channel_id=1, source_target_pairs={{2,0},{3,1},{0,2},{1,3},{6,4},{7,5},{4,6},{5,7},{10,8},{11,9},{8,1... | collective-permute-start | bytes 1572872 | tf_op jit(solution)/shard_map/ppermute | solution.py:36
  37.7 11.9 %collective-permute-done.2.refs_2_ = bf16[64,4096]{1,0:T(8,128)(2,1)} collective-permute-done((bf16[64,4096]{1,0:T(8,128)(2,1)}, bf16[64,4096]{1,0:T(8,128)(2,1)}, u32[]{:S(2)}, u32[]{:S(2)}) %collective-permute-start.2) | collective-permute-done | bytes 524320 | tf_op jit(solution)/shard_map/ppermute | solution.py:36
  49.6 10.8 %collective-permute-done.refs_0_ = bf16[64,4096]{1,0:T(8,128)(2,1)} collective-permute-done((bf16[64,4096]{1,0:T(8,128)(2,1)}, bf16[64,4096]{1,0:T(8,128)(2,1)}, u32[]{:S(2)}, u32[]{:S(2)}) %collective-permute-start) | collective-permute-done | bytes 524320 | tf_op jit(solution)/shard_map/ppermute | solution.py:36
  64.0 1.6 %copy-done.8 = bf16[4096,256]{1,0:T(8,128)(2,1)S(1)} copy-done((bf16[4096,256]{1,0:T(8,128)(2,1)S(1)}, bf16[4096,256]{1,0:T(8,128)(2,1)}, u32[]{:S(2)}) %copy-start.8) | copy-done | bytes 2097176
  65.6 3.4 %shard_map.118 = (bf16[512,256]{1,0:T(8,128)(2,1)S(1)}, bf16[512,256]{1,0:T(8,128)(2,1)S(1)}) custom-call(s32[2]{0:T(128)S(1)} %pad_add_fusion.2.place, bf16[128,4096]{1,0:T(8,128)(2,1)S(1)} %copy-done.1, bf16[128,4096]{1,0:T(8,128)(2,1)} %collective-permute-done.4.refs_1_, f32[1,4096]{1,0:T(1,128)S(1)} %get-tuple-element.36.refs_2_.refs_4_, ...), custom_call_target="tpu_custom_call" | custom-call | flops 1073741824 | bytes 6291456 | tf_op jit(solution)/shard_map/pallas_call | solution.py:149
  69.1 3.2 %shard_map.119 = (bf16[512,256]{1,0:T(8,128)(2,1)S(1)}, bf16[512,256]{1,0:T(8,128)(2,1)S(1)}) custom-call(s32[4]{0:T(128)S(1)} %pad_add_fusion.1.place, bf16[64,4096]{1,0:T(8,128)(2,1)} %collective-permute-done.refs_0_, bf16[64,4096]{1,0:T(8,128)(2,1)S(1)} %collective-permute-done.1.refs_1_, bf16[64,4096]{1,0:T(8,128)(2,1)} %collective-permute-done.2.refs_2_, ...), custom_call_target="tpu_custom_call" | custom-call | flops 1073741824 | bytes 6291456 | tf_op jit(solution)/shard_map/pallas_call | solution.py:149
  73.6 4.7 %collective-permute-start.5 = (bf16[128,256]{1,0:T(8,128)(2,1)S(1)}, bf16[128,256]{1,0:T(8,128)(2,1)S(1)}, u32[]{:S(2)}, u32[]{:S(2)}) collective-permute-start(bf16[128,256]{1,0:T(8,128)(2,1)S(1)} %get-tuple-element.34), channel_id=1, source_target_pairs={{0,4},{4,8},{8,12},{1,5},{5,9},{9,13},{2,6},{6,10},{10,14},{3,7},{... | collective-permute-start | bytes 196616 | tf_op jit(solution)/shard_map/ppermute | solution.py:388
  78.4 4.0 %shard_map.121.refs_4_ = bf16[256,256]{1,0:T(8,128)(2,1)S(1)} custom-call(f32[4]{0:T(128)S(1)} %copy-done.18, bf16[512,256]{1,0:T(8,128)(2,1)S(1)} %get-tuple-element.20.q, bf16[512,256]{1,0:T(8,128)(2,1)S(1)} %get-tuple-element.21.kv, bf16[192,256]{1,0:T(8,128)(2,1)S(1)} %shard_map.120.refs_0_, bf16[192,256]{1,0:T(8,128)(2,1)S(1)} %collective-permute-done.7.refs_1_, ...), custom_call_target="tpu_custom_call" | custom-call | flops 1207959552 | bytes 1048576 | tf_op jit(solution)/shard_map/pallas_call | solution.py:398
  84.2 4.0 %shard_map.122.refs_0_ = bf16[512,256]{1,0:T(8,128)(2,1)S(1)} custom-call(s32[2]{0:T(128)S(1)} %add_convert_fusion.ends, f32[4]{0:T(128)S(1)} %copy-done.18, bf16[512,256]{1,0:T(8,128)(2,1)S(1)} %get-tuple-element.20.q, bf16[512,256]{1,0:T(8,128)(2,1)S(1)} %get-tuple-element.21.kv, bf16[128,256]{1,0:T(8,128)(2,1)S(1)} %collective-permute-done.5.head, ...), custom_call_target="tpu_custom_call" | custom-call | flops 1207959552 | bytes 1048576 | tf_op jit(solution)/shard_map/pallas_call | solution.py:408
  88.2 1.6 %collective-permute-start.11 = (bf16[512,256]{1,0:T(8,128)(2,1)S(1)}, bf16[512,256]{1,0:T(8,128)(2,1)}, u32[]{:S(2)}, u32[]{:S(2)}) collective-permute-start(bf16[512,256]{1,0:T(8,128)(2,1)S(1)} %shard_map.122.refs_0_), channel_id=1, source_target_pairs={{2,0},{3,1},{0,2},{1,3},{6,4},{7,5},{4,6},{5,7},{10,8},{11,9},{8,1... | collective-permute-start | bytes 786440 | tf_op jit(solution)/shard_map/ppermute | solution.py:36
  89.8 1.7 %constant_dynamic-slice_fusion.3 = (bf16[256,1024]{1,0:T(8,128)(2,1)S(1)}, bf16[256,1024]{1,0:T(8,128)(2,1)S(1)}, bf16[256,1024]{1,0:T(8,128)(2,1)S(1)}, bf16[256,1024]{1,0:T(8,128)(2,1)S(1)}) fusion(bf16[1024,1024]{1,0:T(8,128)(2,1)} %param.22, s32[]{:T(128)S(6)} %select_n.134, s32[]{:T(128)S(6)} %select_n.135, s32[]{:T(128)S(6)} %select_n.137, ...), kind=kLoop, calls=%fused_computation.30 | loop fusion | bytes 4194320 | tf_op jit(solution)/shard_map/dynamic_slice | solution.py:424
  91.6 4.9 %collective-permute-done.11.refs_2_ = bf16[512,256]{1,0:T(8,128)(2,1)} collective-permute-done((bf16[512,256]{1,0:T(8,128)(2,1)S(1)}, bf16[512,256]{1,0:T(8,128)(2,1)}, u32[]{:S(2)}, u32[]{:S(2)}) %collective-permute-start.11) | collective-permute-done | bytes 262176 | tf_op jit(solution)/shard_map/ppermute | solution.py:36
  96.8 1.5 %collective-permute-done.12.refs_3_ = bf16[512,256]{1,0:T(8,128)(2,1)S(1)} collective-permute-done((bf16[512,256]{1,0:T(8,128)(2,1)}, bf16[512,256]{1,0:T(8,128)(2,1)S(1)}, u32[]{:S(2)}, u32[]{:S(2)}) %collective-permute-start.12) | collective-permute-done | bytes 262176 | tf_op jit(solution)/shard_map/ppermute | solution.py:40
  98.3 2.4 %shard_map.124 = (bf16[128,1024]{1,0:T(8,128)(2,1)S(1)}, bf16[128,1024]{1,0:T(8,128)(2,1)}) custom-call(s32[2]{0:T(128)S(1)} %pad_add_fusion.2.place, bf16[512,256]{1,0:T(8,128)(2,1)S(1)} %shard_map.122.refs_0_, bf16[512,256]{1,0:T(8,128)(2,1)S(1)} %collective-permute-done.10.refs_1_, bf16[512,256]{1,0:T(8,128)(2,1)} %collective-permute-done.11.refs_2_, ...), custom_call_target="tpu_custom_call" | custom-call | flops 536870912 | bytes 4194304 | tf_op jit(solution)/shard_map/pallas_call | solution.py:273
  101.5 2.4 %shard_map.123 = (bf16[128,1024]{1,0:T(8,128)(2,1)}, bf16[128,1024]{1,0:T(8,128)(2,1)}) custom-call(s32[2]{0:T(128)S(1)} %pad_add_fusion.place, bf16[512,256]{1,0:T(8,128)(2,1)S(1)} %shard_map.122.refs_0_, bf16[512,256]{1,0:T(8,128)(2,1)S(1)} %collective-permute-done.10.refs_1_, bf16[512,256]{1,0:T(8,128)(2,1)} %collective-permute-done.11.refs_2_, ...), custom_call_target="tpu_custom_call" | custom-call | flops 536870912 | bytes 4194304 | tf_op jit(solution)/shard_map/pallas_call | solution.py:273
  103.9 1.5 %collective-permute-start.14 = (bf16[128,1024]{1,0:T(8,128)(2,1)}, bf16[128,1024]{1,0:T(8,128)(2,1)}, u32[]{:S(2)}, u32[]{:S(2)}) collective-permute-start(bf16[128,1024]{1,0:T(8,128)(2,1)} %get-tuple-element.24), channel_id=1, source_target_pairs={{0,2},{1,3},{2,0},{3,1},{4,6},{5,7},{6,4},{7,5},{8,10},{9,11},{10,... | collective-permute-start | bytes 786440 | tf_op jit(solution)/shard_map/ppermute | solution.py:48
  107.3 1.7 %shard_map.126.refs_0_ = bf16[128,4096]{1,0:T(8,128)(2,1)} custom-call(s32[1]{0:T(128)} %bitcast.15.place, bf16[128,4096]{1,0:T(8,128)(2,1)S(1)} %copy-done.1, f32[1,4096]{1,0:T(1,128)S(1)} %get-tuple-element.37.gate, bf16[128,1024]{1,0:T(8,128)(2,1)} %collective-permute-done.15.blend, ...), custom_call_target="tpu_custom_call", output_to_operand_aliasing={{}: (4, {})} | custom-call | flops 1048576 | bytes 1048576 | tf_op jit(solution)/shard_map/pallas_call | solution.py:296
  109.1 4.3 %collective-permute-done.14.blend = bf16[128,1024]{1,0:T(8,128)(2,1)} collective-permute-done((bf16[128,1024]{1,0:T(8,128)(2,1)}, bf16[128,1024]{1,0:T(8,128)(2,1)}, u32[]{:S(2)}, u32[]{:S(2)}) %collective-permute-start.14) | collective-permute-done | bytes 262176 | tf_op jit(solution)/shard_map/ppermute | solution.py:48
  113.3 1.7 %shard_map.127.refs_0_ = bf16[128,4096]{1,0:T(8,128)(2,1)} custom-call(s32[1]{0:T(128)} %bitcast.14.place, bf16[128,4096]{1,0:T(8,128)(2,1)S(1)} %copy-done.1, f32[1,4096]{1,0:T(1,128)S(1)} %get-tuple-element.37.gate, bf16[128,1024]{1,0:T(8,128)(2,1)} %collective-permute-done.14.blend, ...), custom_call_target="tpu_custom_call", output_to_operand_aliasing={{}: (4, {})} | custom-call | flops 1048576 | bytes 1048576 | tf_op jit(solution)/shard_map/pallas_call | solution.py:296
  115.1 2.6 %collective-permute-done.13.blend = bf16[128,1024]{1,0:T(8,128)(2,1)S(1)} collective-permute-done((bf16[128,1024]{1,0:T(8,128)(2,1)}, bf16[128,1024]{1,0:T(8,128)(2,1)S(1)}, u32[]{:S(2)}, u32[]{:S(2)}) %collective-permute-start.13) | collective-permute-done | bytes 262176 | tf_op jit(solution)/shard_map/ppermute | solution.py:48
  (83 shorter events, 22.0 us)
Async XLA Ops:
  2.2 22.3 %copy-start.13 = (f32[4096]{0:T(1024)S(1)}, f32[4096]{0:T(1024)}, u32[]{:S(2)}) copy-start(f32[4096]{0:T(1024)} %param.15) | copy-start | bytes 49156
  3.7 29.7 %copy-start.1 = (bf16[128,4096]{1,0:T(8,128)(2,1)S(1)}, bf16[128,4096]{1,0:T(8,128)(2,1)}, u32[]{:S(2)}) copy-start(bf16[128,4096]{1,0:T(8,128)(2,1)} %latent.7) | copy-start | bytes 3145732
  29.3 49.0 %collective-permute-start.9 = (bf16[192,256]{1,0:T(8,128)(2,1)S(1)}, bf16[192,256]{1,0:T(8,128)(2,1)S(1)}, u32[]{:S(2)}, u32[]{:S(2)}) collective-permute-start(bf16[192,256]{1,0:T(8,128)(2,1)S(1)} %shard_map.120.refs_0_), channel_id=1, source_target_pairs={{12,0},{0,4},{4,8},{8,12},{13,1},{1,5},{5,9},{9,13},{14,2},{2,6},{... | collective-permute-start | bytes 294920 | tf_op jit(solution)/shard_map/ppermute | solution.py:373
  31.0 47.3 %collective-permute-start.8 = (bf16[192,256]{1,0:T(8,128)(2,1)S(1)}, bf16[192,256]{1,0:T(8,128)(2,1)S(1)}, u32[]{:S(2)}, u32[]{:S(2)}) collective-permute-start(bf16[192,256]{1,0:T(8,128)(2,1)S(1)} %shard_map.120.refs_0_), channel_id=1, source_target_pairs={{8,0},{12,4},{0,8},{4,12},{9,1},{13,5},{1,9},{5,13},{10,2},{14,6},... | collective-permute-start | bytes 294920 | tf_op jit(solution)/shard_map/ppermute | solution.py:373
  33.4 28.1 %collective-permute-start.4 = (bf16[128,4096]{1,0:T(8,128)(2,1)S(1)}, bf16[128,4096]{1,0:T(8,128)(2,1)}, u32[]{:S(2)}, u32[]{:S(2)}) collective-permute-start(bf16[128,4096]{1,0:T(8,128)(2,1)S(1)} %copy-done.1), channel_id=1, source_target_pairs={{1,0},{0,1},{3,2},{2,3},{5,4},{4,5},{7,6},{6,7},{9,8},{8,9},{11,10... | collective-permute-start | bytes 3145736 | tf_op jit(solution)/shard_map/ppermute | solution.py:40
  34.5 15.1 %collective-permute-start.2 = (bf16[64,4096]{1,0:T(8,128)(2,1)}, bf16[64,4096]{1,0:T(8,128)(2,1)}, u32[]{:S(2)}, u32[]{:S(2)}) collective-permute-start(bf16[64,4096]{1,0:T(8,128)(2,1)} %get-tuple-element.31), channel_id=1, source_target_pairs={{2,0},{3,1},{0,2},{1,3},{6,4},{7,5},{4,6},{5,7},{10,8},{11,9},{8,1... | collective-permute-start | bytes 1572872 | tf_op jit(solution)/shard_map/ppermute | solution.py:36
  36.0 24.4 %collective-permute-start = (bf16[64,4096]{1,0:T(8,128)(2,1)}, bf16[64,4096]{1,0:T(8,128)(2,1)}, u32[]{:S(2)}, u32[]{:S(2)}) collective-permute-start(bf16[64,4096]{1,0:T(8,128)(2,1)} %get-tuple-element.32), channel_id=1, source_target_pairs={{2,0},{3,1},{0,2},{1,3},{6,4},{7,5},{4,6},{5,7},{10,8},{11,9},{8,1... | collective-permute-start | bytes 1572872 | tf_op jit(solution)/shard_map/ppermute | solution.py:36
  49.6 19.4 %collective-permute-start.3 = (bf16[64,4096]{1,0:T(8,128)(2,1)}, bf16[64,4096]{1,0:T(8,128)(2,1)S(1)}, u32[]{:S(2)}, u32[]{:S(2)}) collective-permute-start(bf16[64,4096]{1,0:T(8,128)(2,1)} %collective-permute-done.2.refs_2_), channel_id=1, source_target_pairs={{1,0},{0,1},{3,2},{2,3},{5,4},{4,5},{7,6},{6,7},{9,8},{8,9},{11,10... | collective-permute-start | bytes 1572872 | tf_op jit(solution)/shard_map/ppermute | solution.py:40
  60.4 8.7 %collective-permute-start.1 = (bf16[64,4096]{1,0:T(8,128)(2,1)}, bf16[64,4096]{1,0:T(8,128)(2,1)S(1)}, u32[]{:S(2)}, u32[]{:S(2)}) collective-permute-start(bf16[64,4096]{1,0:T(8,128)(2,1)} %collective-permute-done.refs_0_), channel_id=1, source_target_pairs={{1,0},{0,1},{3,2},{2,3},{5,4},{4,5},{7,6},{6,7},{9,8},{8,9},{11,10... | collective-permute-start | bytes 1572872 | tf_op jit(solution)/shard_map/ppermute | solution.py:40
  61.5 16.9 %collective-permute-start.7 = (bf16[192,256]{1,0:T(8,128)(2,1)S(1)}, bf16[192,256]{1,0:T(8,128)(2,1)S(1)}, u32[]{:S(2)}, u32[]{:S(2)}) collective-permute-start(bf16[192,256]{1,0:T(8,128)(2,1)S(1)} %shard_map.120.refs_0_), channel_id=1, source_target_pairs={{4,0},{8,4},{12,8},{0,12},{5,1},{9,5},{13,9},{1,13},{6,2},{10,6},{... | collective-permute-start | bytes 294920 | tf_op jit(solution)/shard_map/ppermute | solution.py:373
  65.6 3.4 %copy-start.4 = (bf16[4096,128]{1,0:T(8,128)(2,1)S(1)}, bf16[4096,128]{1,0:T(8,128)(2,1)}, u32[]{:S(2)}) copy-start(bf16[4096,128]{1,0:T(8,128)(2,1)} %wk.1) | copy-start | bytes 3145732
  65.6 3.4 %copy-start.7 = (bf16[4096,128]{1,0:T(8,128)(2,1)S(1)}, bf16[4096,128]{1,0:T(8,128)(2,1)}, u32[]{:S(2)}) copy-start(bf16[4096,128]{1,0:T(8,128)(2,1)} %wv.1) | copy-start | bytes 3145732
  65.6 3.4 %copy-start.9 = (bf16[4096,256]{1,0:T(8,128)(2,1)S(1)}, bf16[4096,256]{1,0:T(8,128)(2,1)}, u32[]{:S(2)}) copy-start(bf16[4096,256]{1,0:T(8,128)(2,1)} %refs_6_.3) | copy-start | bytes 6291460
  69.0 9.3 %copy-start.18 = (f32[4]{0:T(128)S(1)}, f32[4]{0:T(128)}, u32[]{:S(2)}) copy-start(f32[4]{0:T(128)} %sink.3) | copy-start | bytes 52
  72.3 10.1 %collective-permute-start.6 = (bf16[128,256]{1,0:T(8,128)(2,1)S(1)}, bf16[128,256]{1,0:T(8,128)(2,1)S(1)}, u32[]{:S(2)}, u32[]{:S(2)}) collective-permute-start(bf16[128,256]{1,0:T(8,128)(2,1)S(1)} %get-tuple-element.33), channel_id=1, source_target_pairs={{4,0},{8,4},{12,8},{5,1},{9,5},{13,9},{6,2},{10,6},{14,10},{7,3},{... | collective-permute-start | bytes 196616 | tf_op jit(solution)/shard_map/ppermute | solution.py:391
  73.6 8.8 %collective-permute-start.5 = (bf16[128,256]{1,0:T(8,128)(2,1)S(1)}, bf16[128,256]{1,0:T(8,128)(2,1)S(1)}, u32[]{:S(2)}, u32[]{:S(2)}) collective-permute-start(bf16[128,256]{1,0:T(8,128)(2,1)S(1)} %get-tuple-element.34), channel_id=1, source_target_pairs={{0,4},{4,8},{8,12},{1,5},{5,9},{9,13},{2,6},{6,10},{10,14},{3,7},{... | collective-permute-start | bytes 196616 | tf_op jit(solution)/shard_map/ppermute | solution.py:388
  78.3 4.0 %copy-start.14 = (bf16[192,256]{1,0:T(8,128)(2,1)}, bf16[192,256]{1,0:T(8,128)(2,1)S(1)}, u32[]{:S(2)}) copy-start(bf16[192,256]{1,0:T(8,128)(2,1)S(1)} %collective-permute-done.9.refs_3_) | copy-start | bytes 294916
  78.3 4.0 %copy-start.16 = (bf16[192,256]{1,0:T(8,128)(2,1)}, bf16[192,256]{1,0:T(8,128)(2,1)S(1)}, u32[]{:S(2)}) copy-start(bf16[192,256]{1,0:T(8,128)(2,1)S(1)} %collective-permute-done.8.refs_2_) | copy-start | bytes 294916
  88.2 8.3 %collective-permute-start.11 = (bf16[512,256]{1,0:T(8,128)(2,1)S(1)}, bf16[512,256]{1,0:T(8,128)(2,1)}, u32[]{:S(2)}, u32[]{:S(2)}) collective-permute-start(bf16[512,256]{1,0:T(8,128)(2,1)S(1)} %shard_map.122.refs_0_), channel_id=1, source_target_pairs={{2,0},{3,1},{0,2},{1,3},{6,4},{7,5},{4,6},{5,7},{10,8},{11,9},{8,1... | collective-permute-start | bytes 786440 | tf_op jit(solution)/shard_map/ppermute | solution.py:36
  91.5 5.3 %collective-permute-start.10 = (bf16[512,256]{1,0:T(8,128)(2,1)S(1)}, bf16[512,256]{1,0:T(8,128)(2,1)S(1)}, u32[]{:S(2)}, u32[]{:S(2)}) collective-permute-start(bf16[512,256]{1,0:T(8,128)(2,1)S(1)} %shard_map.122.refs_0_), channel_id=1, source_target_pairs={{1,0},{0,1},{3,2},{2,3},{5,4},{4,5},{7,6},{6,7},{9,8},{8,9},{11,10... | collective-permute-start | bytes 786440 | tf_op jit(solution)/shard_map/ppermute | solution.py:40
  96.5 1.7 %collective-permute-start.12 = (bf16[512,256]{1,0:T(8,128)(2,1)}, bf16[512,256]{1,0:T(8,128)(2,1)S(1)}, u32[]{:S(2)}, u32[]{:S(2)}) collective-permute-start(bf16[512,256]{1,0:T(8,128)(2,1)} %collective-permute-done.11.refs_2_), channel_id=1, source_target_pairs={{1,0},{0,1},{3,2},{2,3},{5,4},{4,5},{7,6},{6,7},{9,8},{8,9},{11,10... | collective-permute-start | bytes 786440 | tf_op jit(solution)/shard_map/ppermute | solution.py:40
  101.3 6.0 %collective-permute-start.15 = (bf16[128,1024]{1,0:T(8,128)(2,1)}, bf16[128,1024]{1,0:T(8,128)(2,1)}, u32[]{:S(2)}, u32[]{:S(2)}) collective-permute-start(bf16[128,1024]{1,0:T(8,128)(2,1)} %get-tuple-element.25), channel_id=1, source_target_pairs={{1,0},{0,1},{3,2},{2,3},{5,4},{4,5},{7,6},{6,7},{9,8},{8,9},{11,10... | collective-permute-start | bytes 786440 | tf_op jit(solution)/shard_map/ppermute | solution.py:40
  103.9 9.5 %collective-permute-start.14 = (bf16[128,1024]{1,0:T(8,128)(2,1)}, bf16[128,1024]{1,0:T(8,128)(2,1)}, u32[]{:S(2)}, u32[]{:S(2)}) collective-permute-start(bf16[128,1024]{1,0:T(8,128)(2,1)} %get-tuple-element.24), channel_id=1, source_target_pairs={{0,2},{1,3},{2,0},{3,1},{4,6},{5,7},{6,4},{7,5},{8,10},{9,11},{10,... | collective-permute-start | bytes 786440 | tf_op jit(solution)/shard_map/ppermute | solution.py:48
  105.4 12.3 %collective-permute-start.13 = (bf16[128,1024]{1,0:T(8,128)(2,1)}, bf16[128,1024]{1,0:T(8,128)(2,1)S(1)}, u32[]{:S(2)}, u32[]{:S(2)}) collective-permute-start(bf16[128,1024]{1,0:T(8,128)(2,1)} %get-tuple-element.23), channel_id=1, source_target_pairs={{0,3},{1,2},{2,1},{3,0},{4,7},{5,6},{6,5},{7,4},{8,11},{9,10},{10,... | collective-permute-start | bytes 786440 | tf_op jit(solution)/shard_map/ppermute | solution.py:48
  (13 other events, 16.9 us)
where the time goes:
time: 119 us; the launch traced here: 118 us
  waiting for transfers between devices  36 us (30%)
  Pallas kernels  25.3 us (21%)
  blocking collectives  20.7 us (17%)
  local copies, waits for them, and re-layouts  15.9 us (13%)
  starting transfers between devices  15.8 us (13%)
  other arithmetic  3.4 us (3%)
    ppermute x3, waiting for transfers between devices, from_chip(): return lax.ppermute(block, 'tp', perm)  27.6 us
    all_gather x1, blocking collectives, local(): summed = jnp.sum(lax.all_gather(partial, 'sp', axis=0), axis=0)  15.1 us
    unnamed x42, local copies, waits for them, and re-layouts  13.1 us
    ppermute x2, waiting for transfers between devices, send_rows(): return lax.ppermute(block, 'tp', perm)  6.86 us
    pallas_call x2, Pallas kernels, project(): pl.pallas_call(functools.partial(project_kernel, parts, bool(carried)), o...  6.54 us
    all_gather x1, blocking collectives, local(): vectors = lax.all_gather(summed, 'tp', axis=1, tiled=True)  5.68 us
    pallas_call x4, Pallas kernels, finish(): pl.pallas_call(finish_kernel, out_shape=jax.ShapeDtypeStruct(latent.shape...  5.06 us
    pallas_call x2, Pallas kernels, out_rows(): pl.pallas_call(functools.partial(out_kernel, parts, rows), out_shape=tupl...  4.76 us
  transfers between devices with their start and end apart: 16, of which 6 were waited for; matrix products, arithmetic and copies ran while one was open for 4% of the time, Pallas kernels for 15%

commit v1 on v0

--- a/solution.py
+++ b/solution.py
@@ -46,6 +46,26 @@
         (t, ((t // CORES + step) % chips) * CORES + (t % CORES) ^ flip) for t in range(count)
     ]
     return lax.ppermute(block, "tp", perm)
+
+
+def from_ring(block, ring):
+    if ring > 8:
+        gathered = lax.all_gather(block, "sp", axis=0)
+        return [gathered[i] for i in range(ring)]
+    return [block] + [
+        lax.ppermute(block, "sp", [((i + d) % ring, i) for i in range(ring)])
+        for d in range(1, ring)
+    ]
+
+
+def modulation_kernel(place, norm_gain, *refs):
+    blocks, (gain, shift, gate) = refs[:-3], refs[-3:]
+    width = blocks[0].shape[1]
+    for i, block in enumerate(blocks):
+        cols = pl.ds(pl.multiple_of(place[i], LANES), width)
+        shift[:, cols] = block[0:1, :]
+        gain[:, cols] = norm_gain[:, cols] * (1.0 + block[1:2, :])
+        gate[:, cols] = block[2:3, :]
 
 
 def turn_tables(position):
@@ -353,12 +373,26 @@
         ],
         axis=0,
     )
-    summed = jnp.sum(lax.all_gather(partial, "sp", axis=0), axis=0)
-    vectors = lax.all_gather(summed, "tp", axis=1, tiled=True)
-    vectors, context, rank = lax.optimization_barrier((vectors, context, rank))
-    shift_vec = vectors[0:1]
-    gain_vec = norm_gain[None, :] * (1.0 + vectors[1:2])
-    gate_vec = vectors[2:3]
+    partial, context, rank = lax.optimization_barrier((partial, context, rank))
+    shares = from_ring(partial, ring)
+    summed = functools.reduce(jnp.add, shares)
+    sums = [(summed, index(0, 0)), (from_partner(summed, count), index(0, 1))]
+    for step in range(1, chips):
+        for flip in range(CORES):
+            sums.append((send_rows(summed, count, -step, flip), index(step, flip)))
+    line = jax.ShapeDtypeStruct((1, depth), jnp.float32)
+    gain_vec, shift_vec, gate_vec = pl.pallas_call(
+        modulation_kernel,
+        out_shape=(line, line, line),
+        in_specs=[SMEM] + [VMEM] * (1 + count),
+        out_specs=(VMEM, VMEM, VMEM),
+        compiler_params=pltpu.CompilerParams(vmem_limit_bytes=8 * 1024 * 1024),
+        cost_estimate=cost(2**16, 2**16),
+    )(
+        jnp.stack([at * summed.shape[1] for _, at in sums]),
+        norm_gain[None, :],
+        *[block for block, _ in sums],
+    )
 
     own = pl.pallas_call(
         context_kernel,
@@ -369,10 +403,7 @@
         cost_estimate=cost(4 * context.shape[0] * depth * key_weight.shape[1], 2**22),
     )(context, norm_gain[None, :], key_weight, value_weight)
     if ring <= 8:
-        ctx = [own] + [
-            lax.ppermute(own, "sp", [((i + d) % ring, i) for i in range(ring)])
-            for d in range(1, ring)
-        ]
+        ctx = from_ring(own, ring)
     else:
         ctx = [lax.all_gather(own, "sp", axis=0, tiled=True)]
 

time: 119 us -> 102 us (0.86)
  blocking collectives: 20.7 us -> 0 us
  starting transfers between devices: 15.8 us -> 25.3 us
  local copies, waits for them, and re-layouts: 15.9 us -> 11.6 us
  waiting for transfers between devices: 36 us -> 33.7 us
    all_gather x2 -> x0, blocking collectives: 20.7 us -> none  [the longest x1 15.1 us: local(): summed = jnp.sum(lax.all_gather(partial, 'sp', axis=0), axis=0)]
    ppermute x3 -> x6, starting transfers between devices: 4.19 us -> 11 us  [from_ring(): lax.ppermute(block, 'sp', [((i + d) % ring, i) for i in range(ring)])]
    unnamed x42 -> x32, local copies, waits for them, and re-layouts: 13.1 us -> 8.86 us
    ppermute x3, waiting for transfers between devices: 27.6 us -> 24.4 us  [from_chip(): return lax.ppermute(block, 'tp', perm)]
    ppermute x2 -> x4, starting transfers between devices: 1.73 us -> 3.93 us  [send_rows(): return lax.ppermute(block, 'tp', perm)]
    ppermute x2 -> x4, waiting for transfers between devices: 6.86 us -> 7.8 us  [send_rows(): return lax.ppermute(block, 'tp', perm)]
  transfers between devices with their start and end apart: 16 -> 22, of which waited for: 6 -> 7; matrix products, arithmetic and copies ran while one was open for 4% -> 5% of each run, Pallas kernels for 15% -> 19%
where the time goes in v1:
time: 102 us; the launch traced here: 101 us
  waiting for transfers between devices  33.7 us (33%)
  Pallas kernels  26.2 us (26%)
  starting transfers between devices  25.3 us (25%)
  local copies, waits for them, and re-layouts  11.6 us (11%)
  other arithmetic  3.24 us (3%)
  matrix products  1.14 us (1%)
    ppermute x3, waiting for transfers between devices, from_chip(): return lax.ppermute(block, 'tp', perm)  24.4 us
    ppermute x6, starting transfers between devices, from_ring(): lax.ppermute(block, 'sp', [((i + d) % ring, i) for i in range(ring)])  11 us
    unnamed x32, local copies, waits for them, and re-layouts  8.86 us
    ppermute x4, waiting for transfers between devices, send_rows(): return lax.ppermute(block, 'tp', perm)  7.8 us
    pallas_call x2, Pallas kernels, project(): pl.pallas_call(functools.partial(project_kernel, parts, bool(carried)), o...  6.85 us
    pallas_call x4, Pallas kernels, finish(): pl.pallas_call(finish_kernel, out_shape=jax.ShapeDtypeStruct(latent.shape...  5.07 us
    pallas_call x2, Pallas kernels, out_rows(): pl.pallas_call(functools.partial(out_kernel, parts, rows), out_shape=tupl...  4.81 us
    ppermute x1, starting transfers between devices, local(): lax.ppermute(key_value[row_count - WIN:], 'sp', [(i, i + 1) for i in rang...  4.73 us
  transfers between devices with their start and end apart: 22, of which 7 were waited for; matrix products, arithmetic and copies ran while one was open for 5% of the time, Pallas kernels for 19%

profile of v1, /device:TPU:0, one launch (start us, length us, event | category | flops | bytes accessed | tf_op | source)
XLA Modules:
  0.0 101.5 jit_solution(6140111657321736086)
XLA Ops:
  3.8 3.1 %collective-permute-start.2 = (f32[3,1024]{1,0:T(4,128)S(1)}, f32[3,1024]{1,0:T(4,128)S(1)}, u32[]{:S(2)}, u32[]{:S(2)}) collective-permute-start(f32[3,1024]{1,0:T(4,128)S(1)} %pad_maximum_fusion.1), channel_id=1, source_target_pairs={{12,0},{0,4},{4,8},{8,12},{13,1},{1,5},{5,9},{9,13},{14,2},{2,6},{... | collective-permute-start | bytes 36872 | tf_op jit(solution)/shard_map/ppermute | solution.py:56
  6.9 2.6 %collective-permute-start.1 = (f32[3,1024]{1,0:T(4,128)S(1)}, f32[3,1024]{1,0:T(4,128)S(1)}, u32[]{:S(2)}, u32[]{:S(2)}) collective-permute-start(f32[3,1024]{1,0:T(4,128)S(1)} %pad_maximum_fusion.1), channel_id=1, source_target_pairs={{8,0},{12,4},{0,8},{4,12},{9,1},{13,5},{1,9},{5,13},{10,2},{14,6},... | collective-permute-start | bytes 36872 | tf_op jit(solution)/shard_map/ppermute | solution.py:56
  12.7 1.8 %sine_multiply_fusion = (f32[512,128]{1,0:T(8,128)S(1)}, f32[512,128]{1,0:T(8,128)}) fusion(f32[128]{0:T(128)S(1)} %get-tuple-element.43, f32[128]{0:T(128)S(1)} %get-tuple-element.44, s32[512]{0:T(512)S(1)} %get-tuple-element.45, s32[512]{0:T(512)S(1)} %get-tuple-element.46, pred[128]{0:T(512)(128)(4,1)S(1)} %fusion.8), kind=kLoop, calls=%fused_computation.1 | loop fusion | flops 262144 | bytes 529536 | tf_op jit(solution)/shard_map/mul | solution.py:81
  16.0 9.7 %collective-permute-done.8.refs_2_ = bf16[64,4096]{1,0:T(8,128)(2,1)} collective-permute-done((bf16[64,4096]{1,0:T(8,128)(2,1)}, bf16[64,4096]{1,0:T(8,128)(2,1)}, u32[]{:S(2)}, u32[]{:S(2)}) %collective-permute-start.8) | collective-permute-done | bytes 524320 | tf_op jit(solution)/shard_map/ppermute | solution.py:36
  25.7 10.8 %collective-permute-done.6.refs_0_ = bf16[64,4096]{1,0:T(8,128)(2,1)} collective-permute-done((bf16[64,4096]{1,0:T(8,128)(2,1)}, bf16[64,4096]{1,0:T(8,128)(2,1)}, u32[]{:S(2)}, u32[]{:S(2)}) %collective-permute-start.6) | collective-permute-done | bytes 524320 | tf_op jit(solution)/shard_map/ppermute | solution.py:36
  36.5 1.7 %collective-permute-start.5 = (f32[3,1024]{1,0:T(4,128)S(1)}, f32[3,1024]{1,0:T(4,128)S(1)}, u32[]{:S(2)}, u32[]{:S(2)}) collective-permute-start(f32[3,1024]{1,0:T(4,128)S(1)} %add_add_fusion.refs_0_), channel_id=1, source_target_pairs={{0,3},{1,2},{2,1},{3,0},{4,7},{5,6},{6,5},{7,4},{8,11},{9,10},{10,... | collective-permute-start | bytes 36872 | tf_op jit(solution)/shard_map/ppermute | solution.py:48
  45.2 1.8 %collective-permute-start.14 = (bf16[192,256]{1,0:T(8,128)(2,1)S(1)}, bf16[192,256]{1,0:T(8,128)(2,1)S(1)}, u32[]{:S(2)}, u32[]{:S(2)}) collective-permute-start(bf16[192,256]{1,0:T(8,128)(2,1)S(1)} %shard_map.121.refs_0_), channel_id=1, source_target_pairs={{8,0},{12,4},{0,8},{4,12},{9,1},{13,5},{1,9},{5,13},{10,2},{14,6},... | collective-permute-start | bytes 294920 | tf_op jit(solution)/shard_map/ppermute | solution.py:56
  47.6 2.0 %collective-permute-start.13 = (bf16[192,256]{1,0:T(8,128)(2,1)S(1)}, bf16[192,256]{1,0:T(8,128)(2,1)S(1)}, u32[]{:S(2)}, u32[]{:S(2)}) collective-permute-start(bf16[192,256]{1,0:T(8,128)(2,1)S(1)} %shard_map.121.refs_0_), channel_id=1, source_target_pairs={{4,0},{8,4},{12,8},{0,12},{5,1},{9,5},{13,9},{1,13},{6,2},{10,6},{... | collective-permute-start | bytes 294920 | tf_op jit(solution)/shard_map/ppermute | solution.py:56
  49.6 1.6 %copy-done.6 = bf16[4096,256]{1,0:T(8,128)(2,1)S(1)} copy-done((bf16[4096,256]{1,0:T(8,128)(2,1)S(1)}, bf16[4096,256]{1,0:T(8,128)(2,1)}, u32[]{:S(2)}) %copy-start.6) | copy-done | bytes 2097176
  51.2 3.4 %shard_map.119 = (bf16[512,256]{1,0:T(8,128)(2,1)S(1)}, bf16[512,256]{1,0:T(8,128)(2,1)S(1)}) custom-call(s32[2]{0:T(128)S(1)} %pad_add_fusion.3.place, bf16[128,4096]{1,0:T(8,128)(2,1)S(1)} %copy-done.1, bf16[128,4096]{1,0:T(8,128)(2,1)} %collective-permute-done.10.refs_1_, f32[1,4096]{1,0:T(1,128)S(1)} %get-tuple-element.22.refs_2_.refs_4_, ...), custom_call_target="tpu_custom_call" | custom-call | flops 1073741824 | bytes 6291456 | tf_op jit(solution)/shard_map/pallas_call | solution.py:169
  54.6 3.5 %shard_map.120 = (bf16[512,256]{1,0:T(8,128)(2,1)S(1)}, bf16[512,256]{1,0:T(8,128)(2,1)S(1)}) custom-call(s32[4]{0:T(128)S(1)} %pad_add_fusion.2.place, bf16[64,4096]{1,0:T(8,128)(2,1)} %collective-permute-done.6.refs_0_, bf16[64,4096]{1,0:T(8,128)(2,1)} %collective-permute-done.7.refs_1_, bf16[64,4096]{1,0:T(8,128)(2,1)} %collective-permute-done.8.refs_2_, ...), custom_call_target="tpu_custom_call" | custom-call | flops 1073741824 | bytes 6291456 | tf_op jit(solution)/shard_map/pallas_call | solution.py:169
  59.4 4.7 %collective-permute-start.11 = (bf16[128,256]{1,0:T(8,128)(2,1)S(1)}, bf16[128,256]{1,0:T(8,128)(2,1)S(1)}, u32[]{:S(2)}, u32[]{:S(2)}) collective-permute-start(bf16[128,256]{1,0:T(8,128)(2,1)S(1)} %get-tuple-element.40), channel_id=1, source_target_pairs={{0,4},{4,8},{8,12},{1,5},{5,9},{9,13},{2,6},{6,10},{10,14},{3,7},{... | collective-permute-start | bytes 196616 | tf_op jit(solution)/shard_map/ppermute | solution.py:419
  64.2 4.0 %shard_map.122.refs_4_ = bf16[256,256]{1,0:T(8,128)(2,1)S(1)} custom-call(f32[4]{0:T(128)S(1)} %copy-done.13, bf16[512,256]{1,0:T(8,128)(2,1)S(1)} %get-tuple-element.26.q, bf16[512,256]{1,0:T(8,128)(2,1)S(1)} %get-tuple-element.27.kv, bf16[192,256]{1,0:T(8,128)(2,1)S(1)} %shard_map.121.refs_0_, bf16[192,256]{1,0:T(8,128)(2,1)S(1)} %collective-permute-done.13.refs_1_, ...), custom_call_target="tpu_custom_call" | custom-call | flops 1207959552 | bytes 1048576 | tf_op jit(solution)/shard_map/pallas_call | solution.py:429
  68.2 4.0 %shard_map.123.refs_0_ = bf16[512,256]{1,0:T(8,128)(2,1)S(1)} custom-call(s32[2]{0:T(128)S(1)} %add_convert_fusion.ends, f32[4]{0:T(128)S(1)} %copy-done.13, bf16[512,256]{1,0:T(8,128)(2,1)S(1)} %get-tuple-element.26.q, bf16[512,256]{1,0:T(8,128)(2,1)S(1)} %get-tuple-element.27.kv, bf16[128,256]{1,0:T(8,128)(2,1)S(1)} %collective-permute-done.11.head, ...), custom_call_target="tpu_custom_call" | custom-call | flops 1207959552 | bytes 1048576 | tf_op jit(solution)/shard_map/pallas_call | solution.py:439
  72.2 1.6 %collective-permute-start.17 = (bf16[512,256]{1,0:T(8,128)(2,1)S(1)}, bf16[512,256]{1,0:T(8,128)(2,1)}, u32[]{:S(2)}, u32[]{:S(2)}) collective-permute-start(bf16[512,256]{1,0:T(8,128)(2,1)S(1)} %shard_map.123.refs_0_), channel_id=1, source_target_pairs={{2,0},{3,1},{0,2},{1,3},{6,4},{7,5},{4,6},{5,7},{10,8},{11,9},{8,1... | collective-permute-start | bytes 786440 | tf_op jit(solution)/shard_map/ppermute | solution.py:36
  73.8 1.7 %constant_dynamic-slice_fusion.3 = (bf16[256,1024]{1,0:T(8,128)(2,1)S(1)}, bf16[256,1024]{1,0:T(8,128)(2,1)S(1)}, bf16[256,1024]{1,0:T(8,128)(2,1)S(1)}, bf16[256,1024]{1,0:T(8,128)(2,1)S(1)}) fusion(bf16[1024,1024]{1,0:T(8,128)(2,1)} %param.22, s32[]{:T(128)S(6)} %select_n.142, s32[]{:T(128)S(6)} %select_n.143, s32[]{:T(128)S(6)} %select_n.145, ...), kind=kLoop, calls=%fused_computation.30 | loop fusion | bytes 4194320 | tf_op jit(solution)/shard_map/dynamic_slice | solution.py:455
  75.5 3.9 %collective-permute-done.17.refs_2_ = bf16[512,256]{1,0:T(8,128)(2,1)} collective-permute-done((bf16[512,256]{1,0:T(8,128)(2,1)S(1)}, bf16[512,256]{1,0:T(8,128)(2,1)}, u32[]{:S(2)}, u32[]{:S(2)}) %collective-permute-start.17) | collective-permute-done | bytes 262176 | tf_op jit(solution)/shard_map/ppermute | solution.py:36
  81.2 2.4 %shard_map.125 = (bf16[128,1024]{1,0:T(8,128)(2,1)S(1)}, bf16[128,1024]{1,0:T(8,128)(2,1)}) custom-call(s32[2]{0:T(128)S(1)} %pad_add_fusion.3.place, bf16[512,256]{1,0:T(8,128)(2,1)S(1)} %shard_map.123.refs_0_, bf16[512,256]{1,0:T(8,128)(2,1)S(1)} %collective-permute-done.16.refs_1_, bf16[512,256]{1,0:T(8,128)(2,1)} %collective-permute-done.17.refs_2_, ...), custom_call_target="tpu_custom_call" | custom-call | flops 536870912 | bytes 4194304 | tf_op jit(solution)/shard_map/pallas_call | solution.py:293
  84.5 2.4 %shard_map.124 = (bf16[128,1024]{1,0:T(8,128)(2,1)}, bf16[128,1024]{1,0:T(8,128)(2,1)}) custom-call(s32[2]{0:T(128)S(1)} %pad_add_fusion.1.place, bf16[512,256]{1,0:T(8,128)(2,1)S(1)} %shard_map.123.refs_0_, bf16[512,256]{1,0:T(8,128)(2,1)S(1)} %collective-permute-done.16.refs_1_, bf16[512,256]{1,0:T(8,128)(2,1)} %collective-permute-done.17.refs_2_, ...), custom_call_target="tpu_custom_call" | custom-call | flops 536870912 | bytes 4194304 | tf_op jit(solution)/shard_map/pallas_call | solution.py:293
  86.9 1.5 %collective-permute-start.20 = (bf16[128,1024]{1,0:T(8,128)(2,1)}, bf16[128,1024]{1,0:T(8,128)(2,1)}, u32[]{:S(2)}, u32[]{:S(2)}) collective-permute-start(bf16[128,1024]{1,0:T(8,128)(2,1)} %get-tuple-element.30), channel_id=1, source_target_pairs={{0,2},{1,3},{2,0},{3,1},{4,6},{5,7},{6,4},{7,5},{8,10},{9,11},{10,... | collective-permute-start | bytes 786440 | tf_op jit(solution)/shard_map/ppermute | solution.py:48
  90.3 1.7 %shard_map.127.refs_0_ = bf16[128,4096]{1,0:T(8,128)(2,1)} custom-call(s32[1]{0:T(128)} %bitcast.18.place, bf16[128,4096]{1,0:T(8,128)(2,1)S(1)} %copy-done.1, f32[1,4096]{1,0:T(1,128)S(1)} %get-tuple-element.20.gate, bf16[128,1024]{1,0:T(8,128)(2,1)} %collective-permute-done.21.blend, ...), custom_call_target="tpu_custom_call", output_to_operand_aliasing={{}: (4, {})} | custom-call | flops 1048576 | bytes 1048576 | tf_op jit(solution)/shard_map/pallas_call | solution.py:316
  92.1 4.3 %collective-permute-done.20.blend = bf16[128,1024]{1,0:T(8,128)(2,1)} collective-permute-done((bf16[128,1024]{1,0:T(8,128)(2,1)}, bf16[128,1024]{1,0:T(8,128)(2,1)}, u32[]{:S(2)}, u32[]{:S(2)}) %collective-permute-start.20) | collective-permute-done | bytes 262176 | tf_op jit(solution)/shard_map/ppermute | solution.py:48
  96.4 1.7 %shard_map.128.refs_0_ = bf16[128,4096]{1,0:T(8,128)(2,1)} custom-call(s32[1]{0:T(128)} %bitcast.17.place, bf16[128,4096]{1,0:T(8,128)(2,1)S(1)} %copy-done.1, f32[1,4096]{1,0:T(1,128)S(1)} %get-tuple-element.20.gate, bf16[128,1024]{1,0:T(8,128)(2,1)} %collective-permute-done.20.blend, ...), custom_call_target="tpu_custom_call", output_to_operand_aliasing={{}: (4, {})} | custom-call | flops 1048576 | bytes 1048576 | tf_op jit(solution)/shard_map/pallas_call | solution.py:316
  98.1 2.6 %collective-permute-done.19.blend = bf16[128,1024]{1,0:T(8,128)(2,1)S(1)} collective-permute-done((bf16[128,1024]{1,0:T(8,128)(2,1)}, bf16[128,1024]{1,0:T(8,128)(2,1)S(1)}, u32[]{:S(2)}, u32[]{:S(2)}) %collective-permute-start.19) | collective-permute-done | bytes 262176 | tf_op jit(solution)/shard_map/ppermute | solution.py:48
  (84 shorter events, 22.8 us)
Async XLA Ops:
  3.4 36.9 %copy-start.12 = (f32[4096]{0:T(1024)S(1)}, f32[4096]{0:T(1024)}, u32[]{:S(2)}) copy-start(f32[4096]{0:T(1024)} %param.15) | copy-start | bytes 49156
  3.8 10.8 %collective-permute-start.2 = (f32[3,1024]{1,0:T(4,128)S(1)}, f32[3,1024]{1,0:T(4,128)S(1)}, u32[]{:S(2)}, u32[]{:S(2)}) collective-permute-start(f32[3,1024]{1,0:T(4,128)S(1)} %pad_maximum_fusion.1), channel_id=1, source_target_pairs={{12,0},{0,4},{4,8},{8,12},{13,1},{1,5},{5,9},{9,13},{14,2},{2,6},{... | collective-permute-start | bytes 36872 | tf_op jit(solution)/shard_map/ppermute | solution.py:56
  6.9 29.6 %collective-permute-start.1 = (f32[3,1024]{1,0:T(4,128)S(1)}, f32[3,1024]{1,0:T(4,128)S(1)}, u32[]{:S(2)}, u32[]{:S(2)}) collective-permute-start(f32[3,1024]{1,0:T(4,128)S(1)} %pad_maximum_fusion.1), channel_id=1, source_target_pairs={{8,0},{12,4},{0,8},{4,12},{9,1},{13,5},{1,9},{5,13},{10,2},{14,6},... | collective-permute-start | bytes 36872 | tf_op jit(solution)/shard_map/ppermute | solution.py:56
  9.5 38.2 %collective-permute-start.10 = (bf16[128,4096]{1,0:T(8,128)(2,1)S(1)}, bf16[128,4096]{1,0:T(8,128)(2,1)}, u32[]{:S(2)}, u32[]{:S(2)}) collective-permute-start(bf16[128,4096]{1,0:T(8,128)(2,1)S(1)} %copy-done.1), channel_id=1, source_target_pairs={{1,0},{0,1},{3,2},{2,3},{5,4},{4,5},{7,6},{6,7},{9,8},{8,9},{11,10... | collective-permute-start | bytes 3145736 | tf_op jit(solution)/shard_map/ppermute | solution.py:40
  10.5 15.1 %collective-permute-start.8 = (bf16[64,4096]{1,0:T(8,128)(2,1)}, bf16[64,4096]{1,0:T(8,128)(2,1)}, u32[]{:S(2)}, u32[]{:S(2)}) collective-permute-start(bf16[64,4096]{1,0:T(8,128)(2,1)} %get-tuple-element.37), channel_id=1, source_target_pairs={{2,0},{3,1},{0,2},{1,3},{6,4},{7,5},{4,6},{5,7},{10,8},{11,9},{8,1... | collective-permute-start | bytes 1572872 | tf_op jit(solution)/shard_map/ppermute | solution.py:36
  12.0 24.4 %collective-permute-start.6 = (bf16[64,4096]{1,0:T(8,128)(2,1)}, bf16[64,4096]{1,0:T(8,128)(2,1)}, u32[]{:S(2)}, u32[]{:S(2)}) collective-permute-start(bf16[64,4096]{1,0:T(8,128)(2,1)} %get-tuple-element.38), channel_id=1, source_target_pairs={{2,0},{3,1},{0,2},{1,3},{6,4},{7,5},{4,6},{5,7},{10,8},{11,9},{8,1... | collective-permute-start | bytes 1572872 | tf_op jit(solution)/shard_map/ppermute | solution.py:36
  14.6 21.9 %collective-permute-start = (f32[3,1024]{1,0:T(4,128)S(1)}, f32[3,1024]{1,0:T(4,128)S(1)}, u32[]{:S(2)}, u32[]{:S(2)}) collective-permute-start(f32[3,1024]{1,0:T(4,128)S(1)} %pad_maximum_fusion.1), channel_id=1, source_target_pairs={{4,0},{8,4},{12,8},{0,12},{5,1},{9,5},{13,9},{1,13},{6,2},{10,6},{... | collective-permute-start | bytes 36872 | tf_op jit(solution)/shard_map/ppermute | solution.py:56
  25.7 28.9 %collective-permute-start.9 = (bf16[64,4096]{1,0:T(8,128)(2,1)}, bf16[64,4096]{1,0:T(8,128)(2,1)}, u32[]{:S(2)}, u32[]{:S(2)}) collective-permute-start(bf16[64,4096]{1,0:T(8,128)(2,1)} %collective-permute-done.8.refs_2_), channel_id=1, source_target_pairs={{1,0},{0,1},{3,2},{2,3},{5,4},{4,5},{7,6},{6,7},{9,8},{8,9},{11,10... | collective-permute-start | bytes 1572872 | tf_op jit(solution)/shard_map/ppermute | solution.py:40
  36.4 18.1 %collective-permute-start.7 = (bf16[64,4096]{1,0:T(8,128)(2,1)}, bf16[64,4096]{1,0:T(8,128)(2,1)}, u32[]{:S(2)}, u32[]{:S(2)}) collective-permute-start(bf16[64,4096]{1,0:T(8,128)(2,1)} %collective-permute-done.6.refs_0_), channel_id=1, source_target_pairs={{1,0},{0,1},{3,2},{2,3},{5,4},{4,5},{7,6},{6,7},{9,8},{8,9},{11,10... | collective-permute-start | bytes 1572872 | tf_op jit(solution)/shard_map/ppermute | solution.py:40
  36.5 3.2 %collective-permute-start.5 = (f32[3,1024]{1,0:T(4,128)S(1)}, f32[3,1024]{1,0:T(4,128)S(1)}, u32[]{:S(2)}, u32[]{:S(2)}) collective-permute-start(f32[3,1024]{1,0:T(4,128)S(1)} %add_add_fusion.refs_0_), channel_id=1, source_target_pairs={{0,3},{1,2},{2,1},{3,0},{4,7},{5,6},{6,5},{7,4},{8,11},{9,10},{10,... | collective-permute-start | bytes 36872 | tf_op jit(solution)/shard_map/ppermute | solution.py:48
  38.3 6.8 %collective-permute-start.4 = (f32[3,1024]{1,0:T(4,128)S(1)}, f32[3,1024]{1,0:T(4,128)S(1)}, u32[]{:S(2)}, u32[]{:S(2)}) collective-permute-start(f32[3,1024]{1,0:T(4,128)S(1)} %add_add_fusion.refs_0_), channel_id=1, source_target_pairs={{0,2},{1,3},{2,0},{3,1},{4,6},{5,7},{6,4},{7,5},{8,10},{9,11},{10,... | collective-permute-start | bytes 36872 | tf_op jit(solution)/shard_map/ppermute | solution.py:48
  39.8 5.5 %collective-permute-start.3 = (f32[3,1024]{1,0:T(4,128)S(1)}, f32[3,1024]{1,0:T(4,128)S(1)}, u32[]{:S(2)}, u32[]{:S(2)}) collective-permute-start(f32[3,1024]{1,0:T(4,128)S(1)} %add_add_fusion.refs_0_), channel_id=1, source_target_pairs={{1,0},{0,1},{3,2},{2,3},{5,4},{4,5},{7,6},{6,7},{9,8},{8,9},{11,10... | collective-permute-start | bytes 36872 | tf_op jit(solution)/shard_map/ppermute | solution.py:40
  45.1 19.1 %collective-permute-start.15 = (bf16[192,256]{1,0:T(8,128)(2,1)S(1)}, bf16[192,256]{1,0:T(8,128)(2,1)S(1)}, u32[]{:S(2)}, u32[]{:S(2)}) collective-permute-start(bf16[192,256]{1,0:T(8,128)(2,1)S(1)} %shard_map.121.refs_0_), channel_id=1, source_target_pairs={{12,0},{0,4},{4,8},{8,12},{13,1},{1,5},{5,9},{9,13},{14,2},{2,6},{... | collective-permute-start | bytes 294920 | tf_op jit(solution)/shard_map/ppermute | solution.py:56
  45.2 18.9 %collective-permute-start.14 = (bf16[192,256]{1,0:T(8,128)(2,1)S(1)}, bf16[192,256]{1,0:T(8,128)(2,1)S(1)}, u32[]{:S(2)}, u32[]{:S(2)}) collective-permute-start(bf16[192,256]{1,0:T(8,128)(2,1)S(1)} %shard_map.121.refs_0_), channel_id=1, source_target_pairs={{8,0},{12,4},{0,8},{4,12},{9,1},{13,5},{1,9},{5,13},{10,2},{14,6},... | collective-permute-start | bytes 294920 | tf_op jit(solution)/shard_map/ppermute | solution.py:56
  47.6 16.6 %collective-permute-start.13 = (bf16[192,256]{1,0:T(8,128)(2,1)S(1)}, bf16[192,256]{1,0:T(8,128)(2,1)S(1)}, u32[]{:S(2)}, u32[]{:S(2)}) collective-permute-start(bf16[192,256]{1,0:T(8,128)(2,1)S(1)} %shard_map.121.refs_0_), channel_id=1, source_target_pairs={{4,0},{8,4},{12,8},{0,12},{5,1},{9,5},{13,9},{1,13},{6,2},{10,6},{... | collective-permute-start | bytes 294920 | tf_op jit(solution)/shard_map/ppermute | solution.py:56
  54.6 9.6 %copy-start.13 = (f32[4]{0:T(128)S(1)}, f32[4]{0:T(128)}, u32[]{:S(2)}) copy-start(f32[4]{0:T(128)} %sink.3) | copy-start | bytes 52
  58.1 10.1 %collective-permute-start.12 = (bf16[128,256]{1,0:T(8,128)(2,1)S(1)}, bf16[128,256]{1,0:T(8,128)(2,1)S(1)}, u32[]{:S(2)}, u32[]{:S(2)}) collective-permute-start(bf16[128,256]{1,0:T(8,128)(2,1)S(1)} %get-tuple-element.39), channel_id=1, source_target_pairs={{4,0},{8,4},{12,8},{5,1},{9,5},{13,9},{6,2},{10,6},{14,10},{7,3},{... | collective-permute-start | bytes 196616 | tf_op jit(solution)/shard_map/ppermute | solution.py:422
  59.4 8.8 %collective-permute-start.11 = (bf16[128,256]{1,0:T(8,128)(2,1)S(1)}, bf16[128,256]{1,0:T(8,128)(2,1)S(1)}, u32[]{:S(2)}, u32[]{:S(2)}) collective-permute-start(bf16[128,256]{1,0:T(8,128)(2,1)S(1)} %get-tuple-element.40), channel_id=1, source_target_pairs={{0,4},{4,8},{8,12},{1,5},{5,9},{9,13},{2,6},{6,10},{10,14},{3,7},{... | collective-permute-start | bytes 196616 | tf_op jit(solution)/shard_map/ppermute | solution.py:419
  72.2 7.3 %collective-permute-start.17 = (bf16[512,256]{1,0:T(8,128)(2,1)S(1)}, bf16[512,256]{1,0:T(8,128)(2,1)}, u32[]{:S(2)}, u32[]{:S(2)}) collective-permute-start(bf16[512,256]{1,0:T(8,128)(2,1)S(1)} %shard_map.123.refs_0_), channel_id=1, source_target_pairs={{2,0},{3,1},{0,2},{1,3},{6,4},{7,5},{4,6},{5,7},{10,8},{11,9},{8,1... | collective-permute-start | bytes 786440 | tf_op jit(solution)/shard_map/ppermute | solution.py:36
  75.4 4.3 %collective-permute-start.16 = (bf16[512,256]{1,0:T(8,128)(2,1)S(1)}, bf16[512,256]{1,0:T(8,128)(2,1)S(1)}, u32[]{:S(2)}, u32[]{:S(2)}) collective-permute-start(bf16[512,256]{1,0:T(8,128)(2,1)S(1)} %shard_map.123.refs_0_), channel_id=1, source_target_pairs={{1,0},{0,1},{3,2},{2,3},{5,4},{4,5},{7,6},{6,7},{9,8},{8,9},{11,10... | collective-permute-start | bytes 786440 | tf_op jit(solution)/shard_map/ppermute | solution.py:40
  79.5 1.7 %collective-permute-start.18 = (bf16[512,256]{1,0:T(8,128)(2,1)}, bf16[512,256]{1,0:T(8,128)(2,1)S(1)}, u32[]{:S(2)}, u32[]{:S(2)}) collective-permute-start(bf16[512,256]{1,0:T(8,128)(2,1)} %collective-permute-done.17.refs_2_), channel_id=1, source_target_pairs={{1,0},{0,1},{3,2},{2,3},{5,4},{4,5},{7,6},{6,7},{9,8},{8,9},{11,10... | collective-permute-start | bytes 786440 | tf_op jit(solution)/shard_map/ppermute | solution.py:40
  84.3 6.0 %collective-permute-start.21 = (bf16[128,1024]{1,0:T(8,128)(2,1)}, bf16[128,1024]{1,0:T(8,128)(2,1)}, u32[]{:S(2)}, u32[]{:S(2)}) collective-permute-start(bf16[128,1024]{1,0:T(8,128)(2,1)} %get-tuple-element.31), channel_id=1, source_target_pairs={{1,0},{0,1},{3,2},{2,3},{5,4},{4,5},{7,6},{6,7},{9,8},{8,9},{11,10... | collective-permute-start | bytes 786440 | tf_op jit(solution)/shard_map/ppermute | solution.py:40
  86.9 9.5 %collective-permute-start.20 = (bf16[128,1024]{1,0:T(8,128)(2,1)}, bf16[128,1024]{1,0:T(8,128)(2,1)}, u32[]{:S(2)}, u32[]{:S(2)}) collective-permute-start(bf16[128,1024]{1,0:T(8,128)(2,1)} %get-tuple-element.30), channel_id=1, source_target_pairs={{0,2},{1,3},{2,0},{3,1},{4,6},{5,7},{6,4},{7,5},{8,10},{9,11},{10,... | collective-permute-start | bytes 786440 | tf_op jit(solution)/shard_map/ppermute | solution.py:48
  88.4 12.3 %collective-permute-start.19 = (bf16[128,1024]{1,0:T(8,128)(2,1)}, bf16[128,1024]{1,0:T(8,128)(2,1)S(1)}, u32[]{:S(2)}, u32[]{:S(2)}) collective-permute-start(bf16[128,1024]{1,0:T(8,128)(2,1)} %get-tuple-element.29), channel_id=1, source_target_pairs={{0,3},{1,2},{2,1},{3,0},{4,7},{5,6},{6,5},{7,4},{8,11},{9,10},{10,... | collective-permute-start | bytes 786440 | tf_op jit(solution)/shard_map/ppermute | solution.py:48
  (14 other events, 39.7 us)
